TPU v7x, 32 devices: a whole 2x2x4 slice. The times are simulated.
32 devices in a mesh: sp: 4 (over z), dp: 8 (over y, x, core).
Axes of the slice: x: 2, y: 2, z: 4, core: 2. Of those that a mesh axis runs over, the one named last changes fastest.
Arguments:
- hidden_states: bfloat16 [8, 512, 2048], P('dp', 'sp'), may hold values from -6 to 6
- queries: bfloat16 [8, 512, 2048], P('dp', 'sp'), may hold values from -12 to 12
- key_shift: bfloat16 [8, 512, 16], P('dp', 'sp'), may hold values from -15 to 0
- key_weight: bfloat16 [2048, 256], P('dp'), may hold values from -0.125 to 0.125
- value_weight: bfloat16 [2048, 256], P('dp'), may hold values from -0.125 to 0.125
Outputs:
- attended: bfloat16 [8, 512, 2048], P('dp', 'sp')
All inputs are finite; a program needn't handle non-finite values.
Results may differ from a plain program's by a relative error of at most 0.0079.
Values may be sent and summed in bfloat16 or wider, within the bound.
A program may use at most 64 MiB of HBM per device.

v0:
```python
import jax
import jax.numpy as jnp
from jax import lax
from jax.sharding import PartitionSpec as P

QUERY_HEAD_COUNT = 16
HEAD_DIM = 128


def attend(queries, key_all, value_all, shift_all):
    length, head_count, head_dim = queries.shape
    block_len = min(512, length)
    block_count = length // block_len
    scaling = head_dim ** (-0.5)
    shift_float = shift_all.astype(jnp.float32)
    offsets = jnp.arange(block_len, dtype=jnp.int32)

    def over_queries(block_index, outputs):
        first_row = block_index * block_len
        query_tile = lax.dynamic_slice_in_dim(queries, first_row, block_len, 0)

        def over_keys(back_step, state_pair):
            running, carried = state_pair
            key_start = (block_index - back_step) * block_len
            key_tile = lax.dynamic_slice_in_dim(key_all, key_start, block_len, 0)
            value_tile = lax.dynamic_slice_in_dim(value_all, key_start, block_len, 0)
            shift_tile = lax.dynamic_slice_in_dim(shift_float, key_start, block_len, 0)
            logits = jnp.einsum(
                "qhd,khd->hqk", query_tile, key_tile, preferred_element_type=jnp.float32
            )
            logits = logits * scaling + shift_tile.T[:, None, :]
            visible = (key_start + offsets)[None, :] < (first_row + offsets)[:, None]
            penalty = jnp.where(visible, jax.nn.softplus(logits), 0.0)
            suffix_sum = lax.cumsum(penalty, axis=2, reverse=True) - penalty + carried[:, :, None]
            weights = jnp.where(
                visible, jnp.exp(jax.nn.log_sigmoid(logits) - suffix_sum), 0.0
            ).astype(jnp.bfloat16)
            running = running + jnp.einsum(
                "hqk,khd->hqd", weights, value_tile, preferred_element_type=jnp.float32
            )
            return (running, carried + jnp.sum(penalty, axis=2))

        initial = (
            jnp.zeros((head_count, block_len, head_dim), jnp.float32),
            jnp.zeros((head_count, block_len), jnp.float32),
        )
        running, carried = lax.fori_loop(0, block_index + 1, over_keys, initial)
        finished = jnp.transpose(running, (1, 0, 2)).astype(jnp.bfloat16)
        return lax.dynamic_update_slice_in_dim(outputs, finished, first_row, 0)

    return lax.fori_loop(0, block_count, over_queries, jnp.zeros(queries.shape, jnp.bfloat16))


def per_device(hidden_states, queries, key_shift, key_weight, value_weight):
    seq_local, tok_local, model_dim = hidden_states.shape
    token_rows = hidden_states.reshape(seq_local * tok_local, model_dim)
    key_sum = jnp.dot(
        token_rows,
        lax.all_gather(key_weight, "dp", axis=0, tiled=True),
        preferred_element_type=jnp.float32,
    )
    value_sum = jnp.dot(
        token_rows,
        lax.all_gather(value_weight, "dp", axis=0, tiled=True),
        preferred_element_type=jnp.float32,
    )
    shared_heads = key_weight.shape[1] // HEAD_DIM
    key_local = key_sum.astype(jnp.bfloat16).reshape(seq_local, tok_local, shared_heads, HEAD_DIM)
    value_local = value_sum.astype(jnp.bfloat16).reshape(
        seq_local, tok_local, shared_heads, HEAD_DIM
    )
    query_local = queries.reshape(seq_local, tok_local, QUERY_HEAD_COUNT, HEAD_DIM)
    group_size = QUERY_HEAD_COUNT // shared_heads
    key_wide = jnp.repeat(key_local, group_size, axis=2)
    value_wide = jnp.repeat(value_local, group_size, axis=2)
    query_heads, key_heads, value_heads, shift_heads = (
        lax.all_to_all(query_local, "sp", split_axis=2, concat_axis=1, tiled=True),
        lax.all_to_all(key_wide, "sp", split_axis=2, concat_axis=1, tiled=True),
        lax.all_to_all(value_wide, "sp", split_axis=2, concat_axis=1, tiled=True),
        lax.all_to_all(key_shift, "sp", split_axis=2, concat_axis=1, tiled=True),
    )
    outputs = jax.vmap(attend)(query_heads, key_heads, value_heads, shift_heads)
    returned = lax.all_to_all(outputs, "sp", split_axis=1, concat_axis=2, tiled=True)
    return returned.reshape(seq_local, tok_local, QUERY_HEAD_COUNT * HEAD_DIM)


def solution(mesh):
    placed = (
        P("dp", "sp", None),
        P("dp", "sp", None),
        P("dp", "sp", None),
        P("dp", None),
        P("dp", None),
    )
    return jax.shard_map(
        per_device, mesh=mesh, in_specs=placed, out_specs=P("dp", "sp", None), check_vma=False
    )
```

profile of v0, /device:TPU:0, one launch (start us, length us, event | category | flops | bytes accessed | tf_op | source)
XLA Modules:
  0.0 132.7 jit_solution(17721567945287426333)
XLA Ops:
  6.5 0.7 all-gather.3.cloned.1.call-update
  7.3 0.7 all-gather.5.cloned.1.call-update
  8.0 0.7 copy.54
  9.2 0.7 reduce.9
  10.5 6.3 %all-to-all-start.2 = ((bf16[4,2,256]{2,1,0:T(2,128)(2,1)}), bf16[4,2,256]{2,1,0:T(2,128)(2,1)S(1)}, u32[]{:S(2)}, u32[]{:S(2)}) async-start(bf16[4,2,256]{2,1,0:T(2,128)(2,1)} %reshape.251), calls=%async_computation.2 | async-start | bytes 8192 | tf_op jit(solution)/shard_map/all_to_all | solution.py:80
  16.8 2.0 %copy.32 = bf16[1,128,2048]{1,2,0:T(8,128)(2,1)} copy(bf16[1,128,2048]{2,1,0:T(8,128)(2,1)} %param.8) | data formatting | bytes 1048576 | tf_op args[1]
  18.9 3.4 %all-to-all-done.2 = bf16[4,2,256]{2,1,0:T(2,128)(2,1)S(1)} async-done(((bf16[4,2,256]{2,1,0:T(2,128)(2,1)}), bf16[4,2,256]{2,1,0:T(2,128)(2,1)S(1)}, u32[]{:S(2)}, u32[]{:S(2)}) %all-to-all-start.2) | async-done | bytes 4128 | tf_op jit(solution)/shard_map/all_to_all | solution.py:80
  22.3 3.5 %all-to-all-start = ((bf16[1,128,16,128]{1,3,0,2:T(8,128)(2,1)}), bf16[1,128,16,128]{1,3,0,2:T(8,128)(2,1)S(1)}, u32[]{:S(2)}, u32[]{:S(2)}) async-start(bf16[1,128,16,128]{1,3,0,2:T(8,128)(2,1)} %bitcast.6), calls=%async_computation | async-start | bytes 1048576 | tf_op jit(solution)/shard_map/all_to_all | solution.py:77
  25.8 9.6 %all-gather.3.cloned.1.call-done = bf16[2048,256]{1,0:T(8,128)(2,1)} async-done(((bf16[256,256]{1,0:T(8,128)(2,1)}), bf16[2048,256]{1,0:T(8,128)(2,1)}) %all-gather.3.cloned.1.call-update) | async-done | bytes 1048592 | tf_op jit(solution)/shard_map/all_gather | solution.py:59
  35.4 1.5 %fusion.14 = bf16[16,2,8,128]{3,2,1,0:T(8,128)(2,1)S(1)} fusion(bf16[2048,256]{1,0:T(8,128)(2,1)} %all-gather.3.cloned.1.call-done, bf16[1,128,2048]{2,1,0:T(8,128)(2,1)S(1)} %copy-done), kind=kOutput, calls=%fused_computation.24 | convolution fusion | flops 134250496 | bytes 1638400 | tf_op jit(solution)/shard_map/dot_general | solution.py:57
  36.9 2.3 %all-to-all-done = bf16[1,128,16,128]{1,3,0,2:T(8,128)(2,1)S(1)} async-done(((bf16[1,128,16,128]{1,3,0,2:T(8,128)(2,1)}), bf16[1,128,16,128]{1,3,0,2:T(8,128)(2,1)S(1)}, u32[]{:S(2)}, u32[]{:S(2)}) %all-to-all-start) | async-done | bytes 524320 | tf_op jit(solution)/shard_map/all_to_all | solution.py:77
  39.2 0.9 broadcast_in_dim.36
  40.1 3.5 %all-to-all-start.1 = ((bf16[1,128,16,128]{3,1,0,2:T(8,128)(2,1)}), bf16[1,128,16,128]{3,1,0,2:T(8,128)(2,1)S(1)}, u32[]{:S(2)}, u32[]{:S(2)}) async-start(bf16[1,128,16,128]{3,1,0,2:T(8,128)(2,1)} %bitcast.1), calls=%async_computation.1 | async-start | bytes 1048576 | tf_op jit(solution)/shard_map/all_to_all | solution.py:78
  44.0 16.6 %all-gather.5.cloned.1.call-done = bf16[2048,256]{1,0:T(8,128)(2,1)} async-done(((bf16[256,256]{1,0:T(8,128)(2,1)}), bf16[2048,256]{1,0:T(8,128)(2,1)}) %all-gather.5.cloned.1.call-update) | async-done | bytes 1048592 | tf_op jit(solution)/shard_map/all_gather | solution.py:64
  60.6 1.5 %fusion.15 = bf16[16,2,8,128]{3,2,1,0:T(8,128)(2,1)S(1)} fusion(bf16[2048,256]{1,0:T(8,128)(2,1)} %all-gather.5.cloned.1.call-done, bf16[1,128,2048]{2,1,0:T(8,128)(2,1)S(1)} %copy-done), kind=kOutput, calls=%fused_computation.25 | convolution fusion | flops 134250496 | bytes 1638400 | tf_op jit(solution)/shard_map/dot_general | solution.py:62
  62.2 0.9 broadcast_in_dim.38
  63.1 4.6 %all-to-all-start.3 = ((bf16[1,128,16,128]{3,1,0,2:T(8,128)(2,1)}), bf16[1,128,16,128]{3,1,0,2:T(8,128)(2,1)S(1)}, u32[]{:S(2)}, u32[]{:S(2)}) async-start(bf16[1,128,16,128]{3,1,0,2:T(8,128)(2,1)} %bitcast.21), calls=%async_computation.3 | async-start | bytes 1048576 | tf_op jit(solution)/shard_map/all_to_all | solution.py:79
  67.7 4.4 %fusion.5 = (f32[4,512,512]{1,2,0:T(8,128)S(1)}, f32[4,512,512]{2,1,0:T(8,128)}) fusion(f32[4,512]{1,0:T(4,128)S(1)} %bitcast.103, pred[512,512]{0,1:T(8,128)(4,1)S(1)} %iota_compare_fusion, bf16[512,4,128]{2,0,1:T(8,128)(2,1)S(1)} %bitcast.100, bf16[512,4,128]{2,0,1:T(8,128)(2,1)S(1)} %bitcast.99), kind=kOutput, calls=%fused_computation.7 | convolution fusion | flops 277872640 | bytes 9707520 | tf_op jit(solution)/shard_map/vmap()/while/body/eval_jaxpr/while/body/qhd,khd->hqk/dot_general | solution.py:28
  72.2 19.6 %fusion.11 = f32[1,4,512,4,128]{2,3,4,1,0:T(4,128)S(1)} fusion(f32[1,4,512,4,128]{2,4,3,1,0:T(8,128)S(1)} %bitcast.93), kind=kOutput, calls=%fused_computation.17 | output fusion | flops 133169152 | bytes 8388608 | tf_op jit(solution)/shard_map/reduce-window.8
  91.8 3.3 %copy.38 = f32[1,4,512,4,128]{2,4,3,1,0:T(8,128)} copy(f32[1,4,512,4,128]{2,3,4,1,0:T(4,128)S(1)} %fusion.11) | data formatting | bytes 8388608 | tf_op jit(solution)/shard_map/reduce-window.8
  95.2 8.8 %fusion.4 = bf16[4,512,512]{1,2,0:T(8,128)(2,1)S(1)} fusion(f32[4,512,512]{1,2,0:T(8,128)} %bitcast.92, f32[4,512,512]{2,1,0:T(8,128)} %get-tuple-element.133, f32[4,512]{1,0:T(4,128)S(1)} %bitcast.104, f32[4,512,4]{1,2,0:T(4,128)S(1)} %slice_bitcast_fusion, pred[512,512]{0,1:T(8,128)(4,1)S(1)} %iota_compare_fusion), kind=kLoop, calls=%fused_computation.6 | loop fusion | flops 23068672 | bytes 10788864 | tf_op jit(solution)/shard_map/vmap()/while/body/eval_jaxpr/while/body/convert_element_type | solution.py:37
  104.0 0.9 fusion.13
  105.3 19.2 %all_to_all.78 = bf16[1,512,4,128]{3,2,0,1:T(4,128)(2,1)S(1)} all-to-all(bf16[1,512,4,128]{3,2,0,1:T(4,128)(2,1)S(1)} %copy.42), channel_id=1, replica_groups=mesh['sp'=4,'dp'=8] {'sp'}, dimensions={1} | all-to-all | bytes 1048576 | tf_op jit(solution)/shard_map/all_to_all | solution.py:83
  124.7 1.2 reshape.241
  (22 shorter events, 2.4 us)
Async XLA Ops:
  6.5 28.8 %copy-start = (bf16[1,128,2048]{2,1,0:T(8,128)(2,1)S(1)}, bf16[1,128,2048]{2,1,0:T(8,128)(2,1)}, u32[]{:S(2)}) copy-start(bf16[1,128,2048]{2,1,0:T(8,128)(2,1)} %param.7) | copy-start | bytes 1572868
  6.5 28.8 %all-gather.3.cloned.1.call-start = ((), (), s32[]{:S(2)}) async-start(), calls=%async_computation.5 | async-start | bytes 1179648 | tf_op jit(solution)/shard_map/all_gather | solution.py:59
  7.3 53.4 %all-gather.5.cloned.1.call-start = ((), (), s32[]{:S(2)}) async-start(), calls=%async_computation.6 | async-start | bytes 1179648 | tf_op jit(solution)/shard_map/all_gather | solution.py:64
  10.5 11.8 %all-to-all-start.2 = ((bf16[4,2,256]{2,1,0:T(2,128)(2,1)}), bf16[4,2,256]{2,1,0:T(2,128)(2,1)S(1)}, u32[]{:S(2)}, u32[]{:S(2)}) async-start(bf16[4,2,256]{2,1,0:T(2,128)(2,1)} %reshape.251), calls=%async_computation.2 | async-start | bytes 8192 | tf_op jit(solution)/shard_map/all_to_all | solution.py:80
  22.3 16.9 %all-to-all-start = ((bf16[1,128,16,128]{1,3,0,2:T(8,128)(2,1)}), bf16[1,128,16,128]{1,3,0,2:T(8,128)(2,1)S(1)}, u32[]{:S(2)}, u32[]{:S(2)}) async-start(bf16[1,128,16,128]{1,3,0,2:T(8,128)(2,1)} %bitcast.6), calls=%async_computation | async-start | bytes 1048576 | tf_op jit(solution)/shard_map/all_to_all | solution.py:77
  40.1 22.1 %all-to-all-start.1 = ((bf16[1,128,16,128]{3,1,0,2:T(8,128)(2,1)}), bf16[1,128,16,128]{3,1,0,2:T(8,128)(2,1)S(1)}, u32[]{:S(2)}, u32[]{:S(2)}) async-start(bf16[1,128,16,128]{3,1,0,2:T(8,128)(2,1)} %bitcast.1), calls=%async_computation.1 | async-start | bytes 1048576 | tf_op jit(solution)/shard_map/all_to_all | solution.py:78
  63.1 32.0 %all-to-all-start.3 = ((bf16[1,128,16,128]{3,1,0,2:T(8,128)(2,1)}), bf16[1,128,16,128]{3,1,0,2:T(8,128)(2,1)S(1)}, u32[]{:S(2)}, u32[]{:S(2)}) async-start(bf16[1,128,16,128]{3,1,0,2:T(8,128)(2,1)} %bitcast.21), calls=%async_computation.3 | async-start | bytes 1048576 | tf_op jit(solution)/shard_map/all_to_all | solution.py:79
Sparse Core Ops, SparseCore 0:
  9.2 26.0 all-gather.2
  37.2 23.3 all-gather.4
where the time goes:
time: 133 us
  waiting for transfers between devices  33.3 us (25%)
  other arithmetic  29.2 us (22%)
  blocking collectives  19.2 us (14%)
  starting transfers between devices  17.9 us (13%)
  between operations  13.6 us (10%)
  local copies, waits for them, and re-layouts  11.1 us (8%)
  matrix products  8.43 us (6%)
    another operation x2, other arithmetic  19.6 us
    all_to_all x1, blocking collectives, per_device(): lax.all_to_all(outputs, 'sp', split_axis=1, concat_axis=2, tiled=True)  19.2 us
    all_gather x1, waiting for transfers between devices, per_device(): lax.all_gather(value_weight, 'dp', axis=0, tiled=True)  16.6 us
    all_gather x1, waiting for transfers between devices, per_device(): lax.all_gather(key_weight, 'dp', axis=0, tiled=True)  9.59 us
    convert_element_type x1, other arithmetic, over_keys(): weights = jnp.where(visible, jnp.exp(jax.nn.log_sigmoid(logits) - suffix_...  8.78 us
    all_to_all x1, starting transfers between devices, per_device(): lax.all_to_all(key_shift, 'sp', split_axis=2, concat_axis=1, tiled=True)  6.35 us
    all_to_all x1, starting transfers between devices, per_device(): lax.all_to_all(value_wide, 'sp', split_axis=2, concat_axis=1, tiled=True)  4.6 us
    dot_general x1, matrix products, over_keys(): jnp.einsum('qhd,khd->hqk', query_tile, key_tile, preferred_element_type=j...  4.44 us
  transfers between devices with their start and end apart: 6, of which 4 were waited for; matrix products, arithmetic and copies ran while one was open for 27% of the time, Pallas kernels for 0%

commit v1 on v0

--- a/solution.py
+++ b/solution.py
@@ -77,7 +77,12 @@
         lax.all_to_all(query_local, "sp", split_axis=2, concat_axis=1, tiled=True),
         lax.all_to_all(key_wide, "sp", split_axis=2, concat_axis=1, tiled=True),
         lax.all_to_all(value_wide, "sp", split_axis=2, concat_axis=1, tiled=True),
-        lax.all_to_all(key_shift, "sp", split_axis=2, concat_axis=1, tiled=True),
+        jnp.concatenate(
+            lax.all_to_all(
+                jnp.stack(jnp.split(key_shift, lax.axis_size("sp"), axis=2)), "sp", 0, 0
+            ),
+            axis=1,
+        ),
     )
     outputs = jax.vmap(attend)(query_heads, key_heads, value_heads, shift_heads)
     returned = lax.all_to_all(outputs, "sp", split_axis=1, concat_axis=2, tiled=True)

time: 133 us -> 133 us (level)
    unnamed x7 -> x3, local copies, waits for them, and re-layouts: 3.87 us -> 2.04 us
    another operation x3 -> x4, local copies, waits for them, and re-layouts: 3.28 us -> 4.03 us
    another operation x2 -> x3, other arithmetic: 19.6 us -> 20.2 us
where the time goes in v1:
time: 133 us
  waiting for transfers between devices  34.4 us (26%)
  other arithmetic  29.1 us (22%)
  blocking collectives  19.2 us (14%)
  starting transfers between devices  17.9 us (13%)
  between operations  13.5 us (10%)
  local copies, waits for them, and re-layouts  10.1 us (8%)
  matrix products  8.45 us (6%)
    another operation x2, other arithmetic  19.6 us
    all_to_all x1, blocking collectives, per_device(): lax.all_to_all(outputs, 'sp', split_axis=1, concat_axis=2, tiled=True)  19.2 us
    all_gather x1, waiting for transfers between devices, per_device(): lax.all_gather(value_weight, 'dp', axis=0, tiled=True)  17.7 us
    all_gather x1, waiting for transfers between devices, per_device(): lax.all_gather(key_weight, 'dp', axis=0, tiled=True)  10.6 us
    convert_element_type x1, other arithmetic, over_keys(): weights = jnp.where(visible, jnp.exp(jax.nn.log_sigmoid(logits) - suffix_...  8.78 us
    all_to_all x1, starting transfers between devices, per_device(): lax.all_to_all(jnp.stack(jnp.split(key_shift, lax.axis_size('sp'), axis=2...  6.35 us
    all_to_all x1, starting transfers between devices, per_device(): lax.all_to_all(value_wide, 'sp', split_axis=2, concat_axis=1, tiled=True)  4.6 us
    dot_general x1, matrix products, over_keys(): jnp.einsum('qhd,khd->hqk', query_tile, key_tile, preferred_element_type=j...  4.46 us
  transfers between devices with their start and end apart: 6, of which 4 were waited for; matrix products, arithmetic and copies ran while one was open for 27% of the time, Pallas kernels for 0%

profile of v1, /device:TPU:0, one launch (start us, length us, event | category | flops | bytes accessed | tf_op | source)
XLA Modules:
  0.0 132.7 jit_solution(2154741263389265936)
XLA Ops:
  6.5 0.7 all-gather.3.cloned.1.call-update
  7.3 0.7 all-gather.5.cloned.1.call-update
  8.0 0.8 slice_bitcast_fusion.5
  8.8 0.6 pad_maximum_fusion
  9.4 6.3 %all-to-all-start.2 = ((bf16[4,1,128,4]{2,3,1,0:T(4,128)(2,1)}), bf16[4,1,128,4]{2,3,1,0:T(4,128)(2,1)S(1)}, u32[]{:S(2)}, u32[]{:S(2)}) async-start(bf16[4,1,128,4]{2,3,1,0:T(4,128)(2,1)} %pad_maximum_fusion), calls=%async_computation.2 | async-start | bytes 8192 | tf_op jit(solution)/shard_map/all_to_all | solution.py:81
  15.7 2.0 %copy.32 = bf16[1,128,2048]{1,2,0:T(8,128)(2,1)} copy(bf16[1,128,2048]{2,1,0:T(8,128)(2,1)} %param.8) | data formatting | bytes 1048576 | tf_op args[1]
  17.8 3.5 %all-to-all-done.2 = bf16[4,1,128,4]{2,3,1,0:T(4,128)(2,1)S(1)} async-done(((bf16[4,1,128,4]{2,3,1,0:T(4,128)(2,1)}), bf16[4,1,128,4]{2,3,1,0:T(4,128)(2,1)S(1)}, u32[]{:S(2)}, u32[]{:S(2)}) %all-to-all-start.2) | async-done | bytes 4128 | tf_op jit(solution)/shard_map/all_to_all | solution.py:81
  21.3 3.5 %all-to-all-start = ((bf16[1,128,16,128]{1,3,0,2:T(8,128)(2,1)}), bf16[1,128,16,128]{1,3,0,2:T(8,128)(2,1)S(1)}, u32[]{:S(2)}, u32[]{:S(2)}) async-start(bf16[1,128,16,128]{1,3,0,2:T(8,128)(2,1)} %bitcast.6), calls=%async_computation | async-start | bytes 1048576 | tf_op jit(solution)/shard_map/all_to_all | solution.py:77
  24.8 10.6 %all-gather.3.cloned.1.call-done = bf16[2048,256]{1,0:T(8,128)(2,1)} async-done(((bf16[256,256]{1,0:T(8,128)(2,1)}), bf16[2048,256]{1,0:T(8,128)(2,1)}) %all-gather.3.cloned.1.call-update) | async-done | bytes 1048592 | tf_op jit(solution)/shard_map/all_gather | solution.py:59
  35.4 1.5 %fusion.14 = bf16[16,2,8,128]{3,2,1,0:T(8,128)(2,1)S(1)} fusion(bf16[2048,256]{1,0:T(8,128)(2,1)} %all-gather.3.cloned.1.call-done, bf16[1,128,2048]{2,1,0:T(8,128)(2,1)S(1)} %copy-done), kind=kOutput, calls=%fused_computation.24 | convolution fusion | flops 134250496 | bytes 1638400 | tf_op jit(solution)/shard_map/dot_general | solution.py:57
  36.9 1.2 all-to-all-done
  38.1 0.9 broadcast_in_dim.36
  39.0 3.5 %all-to-all-start.1 = ((bf16[1,128,16,128]{3,1,0,2:T(8,128)(2,1)}), bf16[1,128,16,128]{3,1,0,2:T(8,128)(2,1)S(1)}, u32[]{:S(2)}, u32[]{:S(2)}) async-start(bf16[1,128,16,128]{3,1,0,2:T(8,128)(2,1)} %bitcast.1), calls=%async_computation.1 | async-start | bytes 1048576 | tf_op jit(solution)/shard_map/all_to_all | solution.py:78
  42.9 17.7 %all-gather.5.cloned.1.call-done = bf16[2048,256]{1,0:T(8,128)(2,1)} async-done(((bf16[256,256]{1,0:T(8,128)(2,1)}), bf16[2048,256]{1,0:T(8,128)(2,1)}) %all-gather.5.cloned.1.call-update) | async-done | bytes 1048592 | tf_op jit(solution)/shard_map/all_gather | solution.py:64
  60.6 1.5 %fusion.15 = bf16[16,2,8,128]{3,2,1,0:T(8,128)(2,1)S(1)} fusion(bf16[2048,256]{1,0:T(8,128)(2,1)} %all-gather.5.cloned.1.call-done, bf16[1,128,2048]{2,1,0:T(8,128)(2,1)S(1)} %copy-done), kind=kOutput, calls=%fused_computation.25 | convolution fusion | flops 134250496 | bytes 1638400 | tf_op jit(solution)/shard_map/dot_general | solution.py:62
  62.2 0.9 broadcast_in_dim.38
  63.1 4.6 %all-to-all-start.3 = ((bf16[1,128,16,128]{3,1,0,2:T(8,128)(2,1)}), bf16[1,128,16,128]{3,1,0,2:T(8,128)(2,1)S(1)}, u32[]{:S(2)}, u32[]{:S(2)}) async-start(bf16[1,128,16,128]{3,1,0,2:T(8,128)(2,1)} %bitcast.23), calls=%async_computation.3 | async-start | bytes 1048576 | tf_op jit(solution)/shard_map/all_to_all | solution.py:79
  67.7 4.5 %fusion.5 = (f32[4,512,512]{1,2,0:T(8,128)S(1)}, f32[4,512,512]{2,1,0:T(8,128)}) fusion(f32[4,512]{1,0:T(4,128)S(1)} %convert_bitcast_fusion, pred[512,512]{0,1:T(8,128)(4,1)S(1)} %iota_compare_fusion, bf16[512,4,128]{2,0,1:T(8,128)(2,1)S(1)} %bitcast.101, bf16[512,4,128]{2,0,1:T(8,128)(2,1)S(1)} %bitcast.100), kind=kOutput, calls=%fused_computation.7 | convolution fusion | flops 277872640 | bytes 9707520 | tf_op jit(solution)/shard_map/vmap()/while/body/eval_jaxpr/while/body/qhd,khd->hqk/dot_general | solution.py:28
  72.2 19.6 %fusion.11 = f32[1,4,512,4,128]{2,3,4,1,0:T(4,128)S(1)} fusion(f32[1,4,512,4,128]{2,4,3,1,0:T(8,128)S(1)} %bitcast.94), kind=kOutput, calls=%fused_computation.17 | output fusion | flops 133169152 | bytes 8388608 | tf_op jit(solution)/shard_map/reduce-window.8
  91.8 3.3 %copy.37 = f32[1,4,512,4,128]{2,4,3,1,0:T(8,128)} copy(f32[1,4,512,4,128]{2,3,4,1,0:T(4,128)S(1)} %fusion.11) | data formatting | bytes 8388608 | tf_op jit(solution)/shard_map/reduce-window.8
  95.2 8.8 %fusion.4 = bf16[4,512,512]{1,2,0:T(8,128)(2,1)S(1)} fusion(f32[4,512,512]{1,2,0:T(8,128)} %bitcast.93, f32[4,512,512]{2,1,0:T(8,128)} %get-tuple-element.137, f32[4,512]{1,0:T(4,128)S(1)} %convert_bitcast_fusion, f32[4,512,4]{1,2,0:T(4,128)S(1)} %slice_bitcast_fusion, pred[512,512]{0,1:T(8,128)(4,1)S(1)} %iota_compare_fusion), kind=kLoop, calls=%fused_computation.6 | loop fusion | flops 23068672 | bytes 10788864 | tf_op jit(solution)/shard_map/vmap()/while/body/eval_jaxpr/while/body/convert_element_type | solution.py:37
  104.0 0.9 fusion.13
  105.3 19.2 %all_to_all.74 = bf16[1,512,4,128]{3,2,0,1:T(4,128)(2,1)S(1)} all-to-all(bf16[1,512,4,128]{3,2,0,1:T(4,128)(2,1)S(1)} %copy.41), channel_id=1, replica_groups=mesh['sp'=4,'dp'=8] {'sp'}, dimensions={1} | all-to-all | bytes 1048576 | tf_op jit(solution)/shard_map/all_to_all | solution.py:88
  124.7 1.2 reshape.240
  (19 shorter events, 1.2 us)
Async XLA Ops:
  6.5 28.8 %copy-start = (bf16[1,128,2048]{2,1,0:T(8,128)(2,1)S(1)}, bf16[1,128,2048]{2,1,0:T(8,128)(2,1)}, u32[]{:S(2)}) copy-start(bf16[1,128,2048]{2,1,0:T(8,128)(2,1)} %param.7) | copy-start | bytes 1572868
  6.5 28.8 %all-gather.3.cloned.1.call-start = ((), (), s32[]{:S(2)}) async-start(), calls=%async_computation.5 | async-start | bytes 1179648 | tf_op jit(solution)/shard_map/all_gather | solution.py:59
  7.3 53.4 %all-gather.5.cloned.1.call-start = ((), (), s32[]{:S(2)}) async-start(), calls=%async_computation.6 | async-start | bytes 1179648 | tf_op jit(solution)/shard_map/all_gather | solution.py:64
  9.4 11.9 %all-to-all-start.2 = ((bf16[4,1,128,4]{2,3,1,0:T(4,128)(2,1)}), bf16[4,1,128,4]{2,3,1,0:T(4,128)(2,1)S(1)}, u32[]{:S(2)}, u32[]{:S(2)}) async-start(bf16[4,1,128,4]{2,3,1,0:T(4,128)(2,1)} %pad_maximum_fusion), calls=%async_computation.2 | async-start | bytes 8192 | tf_op jit(solution)/shard_map/all_to_all | solution.py:81
  21.3 16.8 %all-to-all-start = ((bf16[1,128,16,128]{1,3,0,2:T(8,128)(2,1)}), bf16[1,128,16,128]{1,3,0,2:T(8,128)(2,1)S(1)}, u32[]{:S(2)}, u32[]{:S(2)}) async-start(bf16[1,128,16,128]{1,3,0,2:T(8,128)(2,1)} %bitcast.6), calls=%async_computation | async-start | bytes 1048576 | tf_op jit(solution)/shard_map/all_to_all | solution.py:77
  39.0 23.2 %all-to-all-start.1 = ((bf16[1,128,16,128]{3,1,0,2:T(8,128)(2,1)}), bf16[1,128,16,128]{3,1,0,2:T(8,128)(2,1)S(1)}, u32[]{:S(2)}, u32[]{:S(2)}) async-start(bf16[1,128,16,128]{3,1,0,2:T(8,128)(2,1)} %bitcast.1), calls=%async_computation.1 | async-start | bytes 1048576 | tf_op jit(solution)/shard_map/all_to_all | solution.py:78
  63.1 32.0 %all-to-all-start.3 = ((bf16[1,128,16,128]{3,1,0,2:T(8,128)(2,1)}), bf16[1,128,16,128]{3,1,0,2:T(8,128)(2,1)S(1)}, u32[]{:S(2)}, u32[]{:S(2)}) async-start(bf16[1,128,16,128]{3,1,0,2:T(8,128)(2,1)} %bitcast.23), calls=%async_computation.3 | async-start | bytes 1048576 | tf_op jit(solution)/shard_map/all_to_all | solution.py:79
Sparse Core Ops, SparseCore 0:
  9.2 26.0 all-gather.2
  37.2 23.3 all-gather.4
